TPU v7x, 32 devices: a whole 2x2x4 slice. The times are simulated.
32 devices in a mesh: ep: 32 (over z, y, x, core).
Axes of the slice: x: 2, y: 2, z: 4, core: 2. Of those that a mesh axis runs over, the one named last changes fastest.
Arguments:
- latest_embeddings: bfloat16 [512, 2048], P('ep'), may hold values from -6 to 6
- prior_memory_grids: float32 [512, 32, 4096], P('ep'), may hold values from -1.75 to 1.75
- earlier_rescale_gain: float32 [2048], replicated, may hold values from 0.1 to 1.9
- query_map: bfloat16 [2048, 2048], P(None, 'ep'), may hold values from -0.125 to 0.125
- lookup_map: bfloat16 [2048, 2048], P(None, 'ep'), may hold values from -0.125 to 0.125
- content_map: bfloat16 [2048, 2048], P(None, 'ep'), may hold values from -0.125 to 0.125
- forget_lower_map: bfloat16 [2048, 64], replicated, may hold values from -0.125 to 0.125
- forget_upper_map: bfloat16 [64, 2048], replicated, may hold values from -0.75 to 0.75
- forget_shift: float32 [2048], replicated, may hold values from -3 to 3
- adapt_lower_map: bfloat16 [2048, 64], replicated, may hold values from -0.125 to 0.125
- adapt_upper_map: bfloat16 [64, 2048], replicated, may hold values from -0.75 to 0.75
- adapt_shift: float32 [2048], replicated, may hold values from -2 to 2
- erase_lookup_gains: float32 [2048], replicated, may hold values from 0.1 to 1.9
- substitute_lookup_gains: float32 [2048], replicated, may hold values from 0.1 to 1.9
- present_extra_gains: float32 [2048], replicated, may hold values from -1.75 to 1.75
- attender_rescale_gain: float32 [2048], replicated, may hold values from 0.1 to 1.9
- result_map: bfloat16 [2048, 2048], P(None, 'ep'), may hold values from -0.125 to 0.125
- later_rescale_gain: float32 [2048], replicated, may hold values from 0.1 to 1.9
- specialist_switch_maps: bfloat16 [32, 2048, 512], P('ep'), may hold values from -0.125 to 0.125
- specialist_widen_maps: bfloat16 [32, 2048, 512], P('ep'), may hold values from -0.125 to 0.125
- specialist_shrink_maps: bfloat16 [32, 512, 2048], P('ep'), may hold values from -0.25 to 0.25
- picked_specialists: int32 [512, 6], P('ep'), may hold values from 0 to 31, as said below
- specialist_picked_shares: float32 [512, 6], P('ep'), may hold values from 0.02 to 0.5
Outputs:
- new_hidden: bfloat16 [512, 2048], P('ep')
- new_state: float32 [512, 32, 4096], P('ep')
Inputs may be any that keep to these rules, and one draw needn't show every extreme that they name: `picked_specialists`: each row names 6 different experts of one group; a group is a run of 8 consecutive expert numbers. The rows of one device use exactly two groups, one of them for half of the device's rows rounded up and the other for the rest. No expert is named by more than 6 rows of one device, and on every device some expert is named by exactly 6.
All inputs are finite; a program needn't handle non-finite values.
Results may differ from a plain program's by a relative error of at most 0.011.
Values may be sent and summed in bfloat16 or wider, within the bound.
A program may use at most 256 MiB of HBM per device.

v0:
```python
import functools
import math

import jax
import jax.numpy as jnp
from jax import lax
from jax.experimental import pallas as pl
from jax.experimental.pallas import tpu as pltpu
from jax.sharding import PartitionSpec as P

GROUPS = 4
MESH = pl.DeviceIdType.MESH
OUTER = 4

norm_eps = 1e-06
group_eps = 0.00064
unit_eps = 1e-06


def rms_norm(rows_in, gain):
    values = rows_in.astype(jnp.float32)
    scale = lax.rsqrt(jnp.mean(values * values, axis=-1, keepdims=True) + norm_eps)
    return (values * scale * gain).astype(jnp.bfloat16)


def state_kernel(
    q_ref, k_ref, v_ref, dl_ref, al_ref, eg_ref, sg_ref, xg_ref, ag_ref, m_ref,
    mixed_ref, out_ref, sum_ref, spread_ref,
):
    rows, span = q_ref.shape
    repeat = rows // eg_ref.shape[0]
    width = 4 * span
    chunks = m_ref.shape[1] // width
    f32, bf16 = jnp.float32, jnp.bfloat16

    @pl.when(pl.program_id(0) == 0)
    def _():
        shape = sum_ref.shape
        sum_ref[...] = jnp.where(
            lax.broadcasted_iota(jnp.int32, shape, 0) // span
            == lax.broadcasted_iota(jnp.int32, shape, 1),
            1.0, 0.0,
        ).astype(bf16)
        shape = spread_ref.shape
        spread_ref[...] = jnp.where(
            lax.broadcasted_iota(jnp.int32, shape, 1) // span
            == lax.broadcasted_iota(jnp.int32, shape, 0) % span,
            1.0, 0.0,
        ).astype(bf16)

    def gains(ref):
        return jnp.concatenate([ref[...]] * repeat, axis=0)

    def wide(x):
        return jnp.concatenate([x] * 4, axis=1)

    def head_sum(x):
        return jnp.sum(x, axis=-1, keepdims=True)

    q = q_ref[...].astype(f32)
    k = k_ref[...].astype(f32)
    v16 = v_ref[...]
    v = v16.astype(f32)
    decay = jnp.exp(-math.exp(-0.5) * jax.nn.sigmoid(dl_ref[...]))
    rate = jax.nn.sigmoid(al_ref[...])
    erase = k * gains(eg_ref)
    erase = erase * lax.rsqrt(head_sum(erase * erase) + unit_eps)
    repl = k * (1.0 + (rate - 1.0) * gains(sg_ref))
    erase_rate = erase * rate
    erase_w, decay_w, query_w = wide(erase), wide(decay), wide(decay * q)
    removed = jnp.zeros((rows, span), f32)
    kept = jnp.zeros((rows, span), f32)
    for c in range(chunks):
        part = pl.ds(c * width, width)
        m = m_ref[:, part]
        picker = sum_ref[part, :]
        removed += jnp.dot((m * erase_w).astype(bf16), picker, preferred_element_type=f32)
        kept += jnp.dot((m * query_w).astype(bf16), picker, preferred_element_type=f32)
    readout = kept - removed * head_sum(erase_rate * q) + v * head_sum(repl * q)
    centered = readout - jnp.mean(readout, axis=-1, keepdims=True)
    variance = jnp.mean(centered * centered, axis=-1, keepdims=True)
    mixed = centered * lax.rsqrt(variance + group_eps) * gains(ag_ref)
    mixed_ref[...] = (mixed + head_sum(q * repl * gains(xg_ref)) * v).astype(bf16)
    high = removed.astype(bf16)
    low = (removed - high.astype(f32)).astype(bf16)
    both = jnp.concatenate([high, low], axis=1)
    rate_w, repl_w = wide(erase_rate), wide(repl)
    for c in range(chunks):
        part = pl.ds(c * width, width)
        gone = jnp.dot(both, spread_ref[:, part], preferred_element_type=f32)
        added = jnp.dot(v16, spread_ref[:span, part], preferred_element_type=f32)
        out_ref[:, part] = m_ref[:, part] * decay_w - gone * rate_w + added * repl_w


def update_state(q, k, v, decay_logit, rate_logit, gains, state):
    seqs, heads, cells = state.shape
    span = q.shape[1]
    block = 2 * heads
    row = pl.BlockSpec((block, span), lambda i: (i, 0))
    gain = pl.BlockSpec((heads, span), lambda i: (0, 0))
    big = pl.BlockSpec((block, cells), lambda i: (i, 0))
    mixed, new = pl.pallas_call(
        state_kernel,
        grid=(seqs * heads // block,),
        in_specs=[row] * 5 + [gain] * 4 + [big],
        out_specs=[row, big],
        out_shape=[
            jax.ShapeDtypeStruct((seqs * heads, span), jnp.bfloat16),
            jax.ShapeDtypeStruct((seqs * heads, cells), jnp.float32),
        ],
        scratch_shapes=[
            pltpu.VMEM((cells, span), jnp.bfloat16),
            pltpu.VMEM((2 * span, cells), jnp.bfloat16),
        ],
        compiler_params=pltpu.CompilerParams(vmem_limit_bytes=16 * 2**20),
        name="state",
    )(q, k, v, decay_logit, rate_logit, *gains, state.reshape(seqs * heads, cells))
    return mixed, new.reshape(state.shape)


def project_kernel(
    devices, x_ref, w_ref, out_ref, gathered, other, result, landed,
    z_send, z_recv, x_send, x_recv, r_send, r_recv, w_send, w_recv, local_sem,
):
    me = lax.axis_index("ep")
    core, chip = me % 2, me // 2
    partner = me + 1 - 2 * core
    chips = devices // 2
    rows = x_ref.shape[0]
    barrier = pltpu.get_barrier_semaphore()
    pl.semaphore_signal(barrier, inc=1, device_id=(partner,), device_id_type=MESH)

    def greet(k, carry):
        pl.semaphore_signal(
            barrier, inc=1, device_id=((me + 2 * k) % devices,), device_id_type=MESH
        )
        return carry

    lax.fori_loop(1, chips, greet, 0)
    pl.semaphore_wait(barrier, chips)

    inner = chips // OUTER
    layer, place = chip // inner, chip % inner

    def block_of(j):
        return ((layer + OUTER - j) % OUTER) * inner + place

    def outer_copy(j):
        return pltpu.make_async_remote_copy(
            src_ref=x_ref,
            dst_ref=gathered.at[chip],
            send_sem=z_send.at[j],
            recv_sem=z_recv.at[j],
            device_id=((((layer + j) % OUTER) * inner + place) * 2 + core,),
            device_id_type=MESH,
        )

    def inner_copy(j, r):
        block = gathered.at[block_of(j)]
        return pltpu.make_async_remote_copy(
            src_ref=x_ref if j == 0 else block,
            dst_ref=block,
            send_sem=x_send.at[j, r],
            recv_sem=x_recv.at[j, r],
            device_id=((layer * inner + (place + r) % inner) * 2 + core,),
            device_id_type=MESH,
        )

    def inner_start(j):
        def step(r, carry):
            inner_copy(j, r).start()
            return carry
        lax.fori_loop(1, inner, step, 0)

    def inner_finish(j):
        def step(r, carry):
            inner_copy(j, r).wait()
            return carry
        lax.fori_loop(1, inner, step, 0)

    def result_copy(k):
        peer = (me + 2 * k) % devices
        return pltpu.make_async_remote_copy(
            src_ref=result.at[peer // 2],
            dst_ref=landed.at[chip],
            send_sem=r_send.at[k],
            recv_sem=r_recv.at[k],
            device_id=(peer,),
            device_id_type=MESH,
        )

    def start(make):
        def step(k, carry):
            make(k).start()
            return carry
        lax.fori_loop(1, chips, step, 0)

    def finish(make):
        def step(k, carry):
            make(k).wait()
            return carry
        lax.fori_loop(1, chips, step, 0)

    weights = pltpu.make_async_remote_copy(
        src_ref=w_ref,
        dst_ref=other,
        send_sem=w_send,
        recv_sem=w_recv,
        device_id=(partner,),
        device_id_type=MESH,
    )
    for j in range(1, OUTER):
        outer_copy(j).start()
    inner_start(0)
    weights.start()
    mine = pltpu.make_async_copy(x_ref, gathered.at[chip], local_sem)
    mine.start()
    mine.wait()
    for j in range(1, OUTER):
        outer_copy(j).wait_recv()
        inner_start(j)
    weights.wait()
    for j in range(1, OUTER):
        outer_copy(j).wait_send()
    for j in range(OUTER):
        inner_finish(j)
        base = ((layer + OUTER - j) % OUTER) * inner
        tokens = gathered[pl.ds(base, inner)].reshape(inner * rows, x_ref.shape[1])
        for ref, at in ((w_ref, core), (other, 1 - core)):
            product = lax.dot_general(
                tokens, ref[...], (((1,), (1,)), ((), ())), preferred_element_type=jnp.float32
            )
            product = product.astype(jnp.bfloat16)
            for c in range(inner):
                result[base + c, at] = product[c * rows : (c + 1) * rows]
    start(result_copy)
    mine = pltpu.make_async_copy(result.at[chip], landed.at[chip], local_sem)
    mine.start()
    mine.wait()
    finish(result_copy)
    out_ref[...] = landed[...]


def project(x, w, ident):
    devices = lax.axis_size("ep")
    chips = devices // 2
    rows, depth = x.shape
    columns = w.shape[0]
    shape = (chips, 2, rows, columns)
    out = pl.pallas_call(
        functools.partial(project_kernel, devices),
        out_shape=jax.ShapeDtypeStruct(shape, jnp.bfloat16),
        in_specs=[pl.BlockSpec(memory_space=pltpu.VMEM)] * 2,
        out_specs=pl.BlockSpec(memory_space=pltpu.VMEM),
        scratch_shapes=[
            pltpu.VMEM((chips, rows, depth), jnp.bfloat16),
            pltpu.VMEM(w.shape, jnp.bfloat16),
            pltpu.VMEM(shape, jnp.bfloat16),
            pltpu.VMEM(shape, jnp.bfloat16),
            pltpu.SemaphoreType.DMA((OUTER,)),
            pltpu.SemaphoreType.DMA((OUTER,)),
            pltpu.SemaphoreType.DMA((OUTER, chips // OUTER)),
            pltpu.SemaphoreType.DMA((OUTER, chips // OUTER)),
            pltpu.SemaphoreType.DMA((chips,)),
            pltpu.SemaphoreType.DMA((chips,)),
            pltpu.SemaphoreType.DMA,
            pltpu.SemaphoreType.DMA,
            pltpu.SemaphoreType.DMA,
        ],
        compiler_params=pltpu.CompilerParams(
            collective_id=ident, has_side_effects=True, vmem_limit_bytes=20 * 2**20
        ),
        cost_estimate=pl.CostEstimate(
            flops=4 * chips * rows * depth * columns,
            bytes_accessed=32 * chips * rows * depth * 2,
            transcendentals=0,
        ),
        name=f"project{ident}",
    )(x, w)
    return out.reshape(devices, rows, columns)


def exchange_kernel(devices, x_ref, out_ref, landed, send_sem, recv_sem, local_sem):
    me = lax.axis_index("ep")
    barrier = pltpu.get_barrier_semaphore()

    def greet(k, carry):
        pl.semaphore_signal(
            barrier, inc=1, device_id=((me + k) % devices,), device_id_type=MESH
        )
        return carry

    lax.fori_loop(1, devices, greet, 0)
    pl.semaphore_wait(barrier, devices - 1)

    def copy(k):
        peer = (me + k) % devices
        return pltpu.make_async_remote_copy(
            src_ref=x_ref.at[peer],
            dst_ref=landed.at[me],
            send_sem=send_sem.at[k],
            recv_sem=recv_sem.at[k],
            device_id=(peer,),
            device_id_type=MESH,
        )

    def start(k, carry):
        copy(k).start()
        return carry

    def finish(k, carry):
        copy(k).wait()
        return carry

    lax.fori_loop(1, devices, start, 0)
    mine = pltpu.make_async_copy(x_ref.at[me], landed.at[me], local_sem)
    mine.start()
    mine.wait()
    lax.fori_loop(1, devices, finish, 0)
    out_ref[...] = landed[...]


def exchange(x, ident):
    devices = lax.axis_size("ep")
    blocks = x.reshape(devices, -1, 128)
    out = pl.pallas_call(
        functools.partial(exchange_kernel, devices),
        out_shape=jax.ShapeDtypeStruct(blocks.shape, x.dtype),
        in_specs=[pl.BlockSpec(memory_space=pltpu.VMEM)],
        out_specs=pl.BlockSpec(memory_space=pltpu.VMEM),
        scratch_shapes=[
            pltpu.VMEM(blocks.shape, x.dtype),
            pltpu.SemaphoreType.DMA((devices,)),
            pltpu.SemaphoreType.DMA((devices,)),
            pltpu.SemaphoreType.DMA,
        ],
        compiler_params=pltpu.CompilerParams(collective_id=ident, has_side_effects=True),
        name=f"exchange{ident}",
    )(blocks)
    return out.reshape(x.shape)


def local(
    latest_embeddings,
    prior_memory_grids,
    earlier_rescale_gain,
    query_map,
    lookup_map,
    content_map,
    forget_lower_map,
    forget_upper_map,
    forget_shift,
    adapt_lower_map,
    adapt_upper_map,
    adapt_shift,
    erase_lookup_gains,
    substitute_lookup_gains,
    present_extra_gains,
    attender_rescale_gain,
    result_map,
    later_rescale_gain,
    specialist_switch_maps,
    specialist_widen_maps,
    specialist_shrink_maps,
    picked_specialists,
    specialist_picked_shares,
):
    seq_count, model_width = latest_embeddings.shape
    attender_count = prior_memory_grids.shape[1]
    channel_span = model_width // attender_count
    devices = lax.axis_size("ep")
    columns = query_map.shape[1]
    normed = rms_norm(latest_embeddings, earlier_rescale_gain)
    stacked = jnp.concatenate([query_map.T, lookup_map.T, content_map.T], axis=0)
    projected = project(normed, stacked, 0).reshape(devices, seq_count, 3, columns)
    projected = projected.transpose(2, 1, 0, 3).reshape(
        3, seq_count * attender_count, channel_span
    )
    decay_low = jnp.tanh(
        jnp.dot(normed, forget_lower_map, preferred_element_type=jnp.float32)
    ).astype(jnp.bfloat16)
    decay_logit = forget_shift + jnp.dot(
        decay_low, forget_upper_map, preferred_element_type=jnp.float32
    )
    rate_low = jnp.dot(normed, adapt_lower_map, preferred_element_type=jnp.float32).astype(
        jnp.bfloat16
    )
    rate_logit = adapt_shift + jnp.dot(
        rate_low, adapt_upper_map, preferred_element_type=jnp.float32
    )
    mixed, new_state = update_state(
        projected[0],
        projected[1],
        projected[2],
        decay_logit.reshape(-1, channel_span),
        rate_logit.reshape(-1, channel_span),
        [
            gain.reshape(attender_count, channel_span)
            for gain in (
                erase_lookup_gains,
                substitute_lookup_gains,
                present_extra_gains,
                attender_rescale_gain,
            )
        ],
        prior_memory_grids,
    )
    mixer_out = project(mixed.reshape(seq_count, model_width), result_map.T, 1)
    mixer_out = mixer_out.transpose(1, 0, 2).reshape(seq_count, model_width)
    residual = (latest_embeddings.astype(jnp.float32) + mixer_out.astype(jnp.float32)).astype(
        jnp.bfloat16
    )
    second = rms_norm(residual, later_rescale_gain)
    top_count = picked_specialists.shape[1]
    expert_count = specialist_switch_maps.shape[0] * devices
    group_size = expert_count // GROUPS
    capacity = ((seq_count + 1) // 2 * top_count + group_size - 1) // group_size
    flat_ids = picked_specialists.reshape(-1)
    matches = (flat_ids[:, None] == jnp.arange(expert_count, dtype=jnp.int32)[None, :]).astype(
        jnp.int32
    )
    slot_rank = jnp.sum((jnp.cumsum(matches, axis=0) - matches) * matches, axis=1)
    slot_ids = flat_ids * capacity + slot_rank
    picks = (
        slot_ids[:, None] == jnp.arange(expert_count * capacity, dtype=jnp.int32)[None, :]
    ).astype(jnp.bfloat16)
    repeated = jnp.repeat(second, top_count, axis=0)
    send_rows = jnp.einsum("sk,sd->kd", picks, repeated, preferred_element_type=jnp.float32).astype(
        jnp.bfloat16
    )
    send_rows = send_rows.reshape(devices, expert_count // devices * capacity, model_width)
    received = exchange(send_rows, 2)
    rows_in = received.reshape(-1, model_width)
    gate_proj = jnp.dot(rows_in, specialist_switch_maps[0], preferred_element_type=jnp.float32)
    up_proj = jnp.dot(rows_in, specialist_widen_maps[0], preferred_element_type=jnp.float32)
    hidden_act = (jax.nn.silu(gate_proj) * up_proj).astype(jnp.bfloat16)
    results = jnp.dot(
        hidden_act, specialist_shrink_maps[0], preferred_element_type=jnp.float32
    ).astype(jnp.bfloat16)
    returned = exchange(results.reshape(received.shape), 3)
    collected = jnp.dot(
        picks, returned.reshape(-1, model_width), preferred_element_type=jnp.float32
    )
    expert_sum = jnp.sum(
        collected.reshape(seq_count, top_count, model_width) * specialist_picked_shares[:, :, None],
        axis=1,
    )
    new_hidden = (residual.astype(jnp.float32) + expert_sum).astype(jnp.bfloat16)
    return (new_hidden, new_state)


def solution(mesh):
    return jax.shard_map(
        local,
        mesh=mesh,
        in_specs=(
            P("ep", None),
            P("ep", None, None),
            P(),
            P(None, "ep"),
            P(None, "ep"),
            P(None, "ep"),
            P(),
            P(),
            P(),
            P(),
            P(),
            P(),
            P(),
            P(),
            P(),
            P(),
            P(None, "ep"),
            P(),
            P("ep", None, None),
            P("ep", None, None),
            P("ep", None, None),
            P("ep", None),
            P("ep", None),
        ),
        out_specs=(P("ep", None), P("ep", None, None)),
        check_vma=False,
    )
```

profile of v0, /device:TPU:15, one launch (start us, length us, event | category | flops | bytes accessed | tf_op | source)
XLA Modules:
  0.0 133.8 jit_solution(10058981947873117228)
XLA Ops:
  0.6 1.1 fusion.21
  1.8 0.9 fusion.23.x_ref
  2.7 1.2 pad_maximum_fusion.w_ref
  3.9 21.5 %project0.1 = bf16[16,2,16,192]{3,2,1,0:T(8,128)(2,1)S(1)} custom-call(bf16[16,2048]{1,0:T(8,128)(2,1)S(1)} %fusion.23.x_ref, bf16[192,2048]{1,0:T(8,128)(2,1)S(1)} %pad_maximum_fusion.w_ref), custom_call_target="tpu_custom_call" | custom-call | flops 402653184 | bytes 33554432 | tf_op jit(solution)/shard_map/project0/pallas_call | solution.py:250
  25.5 0.1 reshape_reshape.15
  25.6 0.6 fusion.36
  26.5 0.4 convolution_add_fusion.1
  27.1 1.4 %convolution_add_fusion = f32[16,2048]{1,0:T(8,128)S(1)} fusion(bf16[64,2048]{1,0:T(8,128)(2,1)} %param.33, bf16[16,2048]{1,0:T(8,128)(2,1)S(1)} %fusion.23.x_ref, bf16[2048,64]{0,1:T(8,128)(2,1)} %param.32, f32[2048]{0:T(1024)S(1)} %copy-done.8), kind=kOutput, calls=%fused_computation.3 | convolution fusion | flops 8422400 | bytes 729088 | tf_op jit(solution)/shard_map/dot_general | solution.py:388
  28.9 3.4 %copy-done.1 = f32[16,32,4096]{2,1,0:T(8,128)S(1)} copy-done((f32[16,32,4096]{2,1,0:T(8,128)S(1)}, f32[16,32,4096]{2,1,0:T(8,128)}, u32[]{:S(2)}) %copy-start.1) | copy-done | bytes 8388632
  32.3 10.1 %state.1 = (bf16[512,64]{1,0:T(8,128)(2,1)S(1)}, f32[512,4096]{1,0:T(8,128)}) custom-call(bf16[512,64]{1,0:T(8,128)(2,1)S(1)} %bitcast.46, bf16[512,64]{1,0:T(8,128)(2,1)S(1)} %bitcast.47, bf16[512,64]{1,0:T(8,128)(2,1)S(1)} %bitcast.48, f32[512,64]{1,0:T(8,128)S(1)} %reshape.103.dl_ref, f32[512,64]{1,0:T(8,128)S(1)} %reshape.104.al_ref, ...), custom_call_target="tpu_custom_call" | custom-call | tf_op jit(solution)/shard_map/state/pallas_call | solution.py:102
  42.4 0.2 reshape.110.x_ref
  42.6 22.2 %project1.1 = bf16[16,2,16,64]{3,2,1,0:T(8,128)(2,1)S(1)} custom-call(bf16[16,2048]{1,0:T(8,128)(2,1)S(1)} %reshape.110.x_ref, bf16[64,2048]{1,0:T(8,128)(2,1)S(1)} %bitcast.49), custom_call_target="tpu_custom_call" | custom-call | flops 134217728 | bytes 33554432 | tf_op jit(solution)/shard_map/project1/pallas_call | solution.py:250
  65.9 0.2 select_reduce_fusion
  66.1 0.5 convolution_convert_fusion.1
  66.6 1.2 reshape_reshape.16.x_ref
  67.8 29.4 %exchange2.1 = bf16[32,96,128]{2,1,0:T(8,128)(2,1)} custom-call(bf16[32,96,128]{2,1,0:T(8,128)(2,1)} %reshape_reshape.16.x_ref), custom_call_target="tpu_custom_call" | custom-call | tf_op jit(solution)/shard_map/exchange2/pallas_call | solution.py:326
  97.2 1.4 %reshape_reshape.17 = bf16[192,2048]{1,0:T(8,128)(2,1)S(1)} reshape(bf16[32,96,128]{2,1,0:T(8,128)(2,1)} %exchange2.1) | data formatting | bytes 1572864 | tf_op jit(solution)/shard_map/reshape;reshape | solution.py:433
  98.7 2.2 %fusion.3 = f32[192,512]{1,0:T(8,128)S(1)} fusion(bf16[192,2048]{1,0:T(8,128)(2,1)S(1)} %reshape_reshape.17, bf16[1,2048,512]{2,1,0:T(8,128)(2,1)} %param.41), kind=kOutput, calls=%fused_computation.8 | convolution fusion | flops 402653184 | bytes 3276800 | tf_op jit(solution)/shard_map/dot_general | solution.py:434
  100.9 3.6 %convolution_convert_fusion = bf16[192,2048]{1,0:T(8,128)(2,1)} fusion(bf16[1,512,2048]{2,1,0:T(8,128)(2,1)S(1)} %copy-done, bf16[192,2048]{1,0:T(8,128)(2,1)S(1)} %reshape_reshape.17, bf16[1,2048,512]{2,1,0:T(8,128)(2,1)} %param.42, f32[192,512]{1,0:T(8,128)S(1)} %fusion.3), kind=kOutput, calls=%fused_computation | convolution fusion | flops 806289408 | bytes 6160384 | tf_op jit(solution)/shard_map/dot_general | solution.py:437
  104.5 2.2 %reshape_reshape.18.x_ref = bf16[32,96,128]{2,1,0:T(8,128)(2,1)} reshape(bf16[192,2048]{1,0:T(8,128)(2,1)} %convolution_convert_fusion) | data formatting | bytes 1572864 | tf_op jit(solution)/shard_map/reshape;reshape | solution.py:325
  106.6 24.6 %exchange3.1 = bf16[32,96,128]{2,1,0:T(8,128)(2,1)} custom-call(bf16[32,96,128]{2,1,0:T(8,128)(2,1)} %reshape_reshape.18.x_ref), custom_call_target="tpu_custom_call" | custom-call | tf_op jit(solution)/shard_map/exchange3/pallas_call | solution.py:326
  131.3 1.4 %reshape.115 = bf16[192,2048,1]{1,0,2:T(8,128)(2,1)S(1)} reshape(bf16[32,96,128]{2,1,0:T(8,128)(2,1)} %exchange3.1) | data formatting | bytes 1572864 | tf_op jit(solution)/shard_map/reshape;reshape | solution.py:442
  132.9 0.3 fusion.5
  133.2 0.6 fusion.28
  (55 shorter events, 2.1 us)
Async XLA Ops:
  0.6 100.2 %copy-start = (bf16[1,512,2048]{2,1,0:T(8,128)(2,1)S(1)}, bf16[1,512,2048]{2,1,0:T(8,128)(2,1)}, u32[]{:S(2)}) copy-start(bf16[1,512,2048]{2,1,0:T(8,128)(2,1)} %param.43) | copy-start | bytes 6291460
  25.4 1.1 copy-start.4
  25.4 1.1 copy-start.5
  25.4 1.1 copy-start.7
  25.6 1.4 %copy-start.8 = (f32[2048]{0:T(1024)S(1)}, f32[2048]{0:T(1024)}, u32[]{:S(2)}) copy-start(f32[2048]{0:T(1024)} %param.34) | copy-start | bytes 24580
  26.2 2.4 %copy-start.9 = (f32[2048]{0:T(1024)S(1)}, f32[2048]{0:T(1024)}, u32[]{:S(2)}) copy-start(f32[2048]{0:T(1024)} %param.35) | copy-start | bytes 24580
  26.2 2.5 %copy-start.10 = (f32[2048]{0:T(1024)S(1)}, f32[2048]{0:T(1024)}, u32[]{:S(2)}) copy-start(f32[2048]{0:T(1024)} %param.36) | copy-start | bytes 24580
  26.2 2.5 %copy-start.11 = (f32[2048]{0:T(1024)S(1)}, f32[2048]{0:T(1024)}, u32[]{:S(2)}) copy-start(f32[2048]{0:T(1024)} %param.37) | copy-start | bytes 24580
  26.2 2.6 %copy-start.12 = (f32[2048]{0:T(1024)S(1)}, f32[2048]{0:T(1024)}, u32[]{:S(2)}) copy-start(f32[2048]{0:T(1024)} %param.38) | copy-start | bytes 24580
  28.9 3.4 %copy-start.1 = (f32[16,32,4096]{2,1,0:T(8,128)S(1)}, f32[16,32,4096]{2,1,0:T(8,128)}, u32[]{:S(2)}) copy-start(f32[16,32,4096]{2,1,0:T(8,128)} %param.24) | copy-start | bytes 25165828
  32.3 10.3 %copy-start.2 = (bf16[2048,64]{0,1:T(8,128)(2,1)S(1)}, bf16[2048,64]{0,1:T(8,128)(2,1)}, u32[]{:S(2)}) copy-start(bf16[2048,64]{0,1:T(8,128)(2,1)} %param.39) | copy-start | bytes 786436
  32.3 32.7 %copy-start.3 = (bf16[16,2048]{1,0:T(8,128)(2,1)S(1)}, bf16[16,2048]{1,0:T(8,128)(2,1)}, u32[]{:S(2)}) copy-start(bf16[16,2048]{1,0:T(8,128)(2,1)} %param.23) | copy-start | bytes 196612
  42.4 22.8 %copy-start.13 = (f32[2048]{0:T(1024)S(1)}, f32[2048]{0:T(1024)}, u32[]{:S(2)}) copy-start(f32[2048]{0:T(1024)} %param.40) | copy-start | bytes 24580
  42.4 23.1 %copy-start.6 = (s32[16,6]{0,1:T(8,128)S(1)}, s32[16,6]{0,1:T(8,128)}, u32[]{:S(2)}) copy-start(s32[16,6]{0,1:T(8,128)} %param.44) | copy-start | bytes 1156
  104.5 28.4 %copy-start.14 = (f32[16,6]{0,1:T(8,128)S(1)}, f32[16,6]{0,1:T(8,128)}, u32[]{:S(2)}) copy-start(f32[16,6]{0,1:T(8,128)} %param.45) | copy-start | bytes 1156
where the time goes:
time: 134 us
  Pallas kernels  108 us (81%)
  local copies, waits for them, and re-layouts  12.1 us (9%)
  matrix products  8.37 us (6%)
  other arithmetic  4.54 us (3%)
    pallas_call x2, Pallas kernels, exchange(): pl.pallas_call(functools.partial(exchange_kernel, devices), out_shape=jax...  54 us
    pallas_call x2, Pallas kernels, project(): pl.pallas_call(functools.partial(project_kernel, devices), out_shape=jax....  43.7 us
    pallas_call x1, Pallas kernels, update_state(): pl.pallas_call(state_kernel, grid=(seqs * heads // block,), in_specs=[row...  10.1 us
    dot_general x1, matrix products, local(): jnp.dot(hidden_act, specialist_shrink_maps[0], preferred_element_type=jnp...  3.59 us
    unnamed x31, local copies, waits for them, and re-layouts  3.55 us
    another operation x2, local copies, waits for them, and re-layouts, exchange(): blocks = x.reshape(devices, -1, 128)  3.44 us

commit v1 on v0

v1 whole, which is shorter than its diff:
```python
import functools
import math

import jax
import jax.numpy as jnp
from jax import lax
from jax.experimental import pallas as pl
from jax.experimental.pallas import tpu as pltpu
from jax.sharding import PartitionSpec as P

GROUPS = 4
MESH = pl.DeviceIdType.MESH
HEAD_PAD = 8

norm_eps = 1e-06
group_eps = 0.00064
unit_eps = 1e-06

f32, bf16 = jnp.float32, jnp.bfloat16


def matmul_t(a, b):
    return lax.dot_general(a, b, (((1,), (1,)), ((), ())), preferred_element_type=f32)


def matmul(a, b):
    return jnp.dot(a, b, preferred_element_type=f32)


def iota(shape, axis):
    return lax.broadcasted_iota(jnp.int32, shape, axis)


def layer_kernel(
    devices,
    x_hbm, m_hbm, wq_hbm, wk_hbm, wv_hbm, wo_hbm, fl_hbm, fu_hbm, al_hbm, au_hbm,
    vec0, vec1, vec2, vec3, vec4, vec5, vec6, vec7,
    wg_hbm, wu_hbm, wd_hbm, pick_hbm, share_hbm,
    hid_ref, m_ref,
    tok, mix, wall, wo, low, vecs, picks, shares, wgb, wub, wdb,
    picker, spread, gains, rows_s, own_s, rem_s, result, landed, xcol, rescol,
    resland, rmsg, zsrc, disp, acc, sshare, part, pland, retsrc, rland,
    loc, psem_s, psem_r,
    az_s, az_r, au_s, au_r, aw_s, aw_r,
    bz_s, bz_r, bu_s, bu_r, bw_s, bw_r,
    cz_s, cz_r, cu_s, cu_r, cw_s, cw_r,
    ret_s, ret_r, msg_s, msg_r, res_s, res_r, sum_s, sum_r, home_s, home_r,
):
    me = lax.axis_index("ep")
    core, chip = me % 2, me // 2
    chips = devices // 2
    inner = chips // GROUPS
    side = math.isqrt(inner)
    layer, place = chip // inner, chip % inner
    along_y, along_x = place // side, place % side
    u = along_x * (1 - core) + along_y * core
    w = along_y * (1 - core) + along_x * core
    vp = w * side + u
    own = layer * inner + vp
    rows, depth = x_hbm.shape
    heads = m_hbm.shape[0] // rows
    span = depth // heads
    cells = m_hbm.shape[1]
    cw = depth // chips
    half = (rows + 1) // 2
    slots = inner * half
    group = devices // GROUPS
    pitch = heads + HEAD_PAD
    fe = wg_hbm.shape[2]

    def place_of(w_, u_):
        return (1 - core) * (w_ * side + u_) + core * (u_ * side + w_)

    def dev(l, w_, u_):
        return ((l * inner + place_of(w_, u_)) * 2 + core,)

    def lyr(j):
        return (layer + GROUPS - j) % GROUPS

    def rdma(src, dst, ss, rs, to):
        return pltpu.make_async_remote_copy(
            src_ref=src, dst_ref=dst, send_sem=ss, recv_sem=rs, device_id=to, device_id_type=MESH
        )

    partner = (me + 1 - 2 * core,)

    local = [(x_hbm, tok.at[own])]
    for i, ref in enumerate((wq_hbm, wk_hbm, wv_hbm)):
        local.append((ref, wall.at[i, core]))
    for i, ref in enumerate((fl_hbm, al_hbm, fu_hbm, au_hbm)):
        local.append((ref, low.at[i]))
    for i, ref in enumerate((vec0, vec1, vec2, vec3, vec4, vec5, vec6, vec7)):
        local.append((ref, vecs.at[pl.ds(i, 1)]))
    local += [(pick_hbm, picks), (share_hbm, shares), (wo_hbm, wo.at[core])]
    early = len(local)
    local.append((m_hbm, m_ref))
    for ref, buf in ((wg_hbm, wgb), (wu_hbm, wub), (wd_hbm, wdb)):
        local.append((ref.at[0], buf.at[core]))
    local = [pltpu.make_async_copy(s, d, loc.at[i]) for i, (s, d) in enumerate(local)]
    swaps = []
    for i, ref in enumerate((wq_hbm, wk_hbm, wv_hbm)):
        swaps.append((ref, wall.at[i, core]))
    swaps.append((wo_hbm, wo.at[core]))
    for ref, buf in ((wg_hbm, wgb), (wu_hbm, wub), (wd_hbm, wdb)):
        swaps.append((ref.at[0], buf.at[core]))
    swaps = [
        rdma(s, d, psem_s.at[i], psem_r.at[i], partner) for i, (s, d) in enumerate(swaps)
    ]

    for copy in local:
        copy.start()
    barrier = pltpu.get_barrier_semaphore()
    pl.semaphore_signal(barrier, inc=1, device_id=partner, device_id_type=MESH)

    def greet(k, carry):
        pl.semaphore_signal(
            barrier, inc=1, device_id=((me + 2 * k) % devices,), device_id_type=MESH
        )
        return carry

    lax.fori_loop(1, chips, greet, 0)

    def z_copy(buf, ss, rs, j):
        return rdma(buf.at[own], buf.at[own], ss.at[j], rs.at[j], dev((layer + j) % GROUPS, w, u))

    def u_copy(buf, ss, rs, j, r):
        block = buf.at[lyr(j) * inner + vp]
        return rdma(block, block, ss.at[j, r], rs.at[j, r], dev(layer, w, (u + r) % side))

    def w_copy(buf, ss, rs, j, r):
        block = buf.at[pl.ds(lyr(j) * inner + w * side, side)]
        return rdma(block, block, ss.at[j, r], rs.at[j, r], dev(layer, (w + r) % side, u))

    def u_start(buf, ss, rs, j):
        for r in range(1, side):
            u_copy(buf, ss, rs, j, r).start()

    def u_to_w(buf, us, ur, ws, wr, j):
        for r in range(1, side):
            u_copy(buf, us, ur, j, r).wait_recv()
        for r in range(1, side):
            w_copy(buf, ws, wr, j, r).start()

    def w_wait(buf, ws, wr, j):
        for r in range(1, side):
            w_copy(buf, ws, wr, j, r).wait_recv()

    def sends_done(buf, us, ur, ws, wr):
        for j in range(GROUPS):
            for r in range(1, side):
                u_copy(buf, us, ur, j, r).wait_send()
                w_copy(buf, ws, wr, j, r).wait_send()

    def spread_copy(src_of, dst, ss, rs, j, k):
        a, b = k // side, k % side
        l2, w2, u2 = lyr(j), (w + a) % side, (u + b) % side
        at = j * inner + k
        return rdma(src_of(l2, w2, u2), dst, ss.at[at], rs.at[at], dev(l2, w2, u2))

    def each(j, fn):
        def step(k, carry):
            fn(k)
            return carry

        lax.fori_loop(1 if j == 0 else 0, inner, step, 0)

    local[0].wait()
    pl.semaphore_wait(barrier, chips)
    for j in range(1, GROUPS):
        z_copy(tok, az_s, az_r, j).start()
    u_start(tok, au_s, au_r, 0)
    for i in range(4):
        swaps[i].start()
    for i in range(1, early):
        local[i].wait()

    lane = iota((1, 2 * span), 1)
    low_lane = lane < span

    shape = picker.shape
    picker[...] = jnp.where(iota(shape, 0) // span == iota(shape, 1) % span, 1.0, 0.0).astype(bf16)
    shape = spread.shape
    spread[...] = jnp.where(iota(shape, 1) // span == iota(shape, 0) % span, 1.0, 0.0).astype(bf16)

    def both_heads(tile):
        turned = pltpu.roll(tile, span, 1)
        return jnp.where(low_lane, tile, turned), jnp.where(low_lane, turned, tile)

    for i in range(4):
        for h in range(heads // 2):
            first, second = both_heads(vecs[3 + i : 4 + i, 2 * h * span : 2 * (h + 1) * span])
            gains[i, 2 * h : 2 * h + 1, :] = first
            gains[i, 2 * h + 1 : 2 * h + 2, :] = second

    def to_rows(slot, h, tile):
        first, second = both_heads(tile)
        rows_s[slot, pl.ds(2 * h, rows, stride=pitch), :] = first
        rows_s[slot, pl.ds(2 * h + 1, rows, stride=pitch), :] = second

    def normed_of(values, gain):
        values = values.astype(f32)
        scale = lax.rsqrt(jnp.mean(values * values, axis=-1, keepdims=True) + norm_eps)
        return (values * scale * gain).astype(bf16)

    mine = normed_of(tok[own], vecs[0:1, :])
    decay_low = jnp.tanh(matmul_t(mine, low[0])).astype(bf16)
    rate_low = matmul_t(mine, low[1]).astype(bf16)
    decay_all = vecs[1:2, :] + matmul(decay_low, low[2])
    rate_all = vecs[2:3, :] + matmul(rate_low, low[3])
    for h in range(heads // 2):
        part_at = slice(2 * h * span, 2 * (h + 1) * span)
        to_rows(3, h, decay_all[:, part_at])
        to_rows(4, h, rate_all[:, part_at])

    top = picks.shape[0]
    chosen = picks[...]
    weight = shares[...]
    eye = iota((rows, rows), 0) == iota((rows, rows), 1)
    before = iota((rows, rows), 0) < iota((rows, rows), 1)
    group_row = jnp.zeros((1, rows), f32)
    for g in range(1, GROUPS):
        group_row += jnp.where(chosen[0:1, :] >= g * group, 1.0, 0.0)

    def to_column(row):
        return jnp.sum(jnp.where(eye, jnp.broadcast_to(row, (rows, rows)), 0.0), axis=1, keepdims=True)

    group_col = to_column(group_row)
    rank_row = jnp.sum(
        jnp.where(jnp.logical_and(group_col == group_row, before), 1.0, 0.0), axis=0, keepdims=True
    )
    home_col = to_column(group_row * half + rank_row)
    per_tile = 128 // rows
    here = iota((1, 128), 1) // rows == vp % per_tile

    def placed(values):
        tiled = jnp.concatenate([values] * per_tile, axis=1)
        return jnp.where(here, tiled, 0.0)

    code = group_row * slots + (vp * half).astype(f32) + rank_row + 1.0
    local_ids = chosen.astype(f32) - group_row * group
    expert = iota((group, rows), 0).astype(f32)
    table = jnp.zeros((group, rows), f32)
    for t in range(top):
        table += jnp.where(expert == local_ids[t : t + 1, :], weight[t : t + 1, :], 0.0)
    rmsg[own, 0:8, :] = jnp.broadcast_to(placed(code), (8, 128))
    rmsg[own, 8 : 8 + group, :] = placed(table)

    per_step = min(inner, 4)

    def project_in(j):
        base = lyr(j) * inner

        def step(s, carry):
            at = base + s * per_step
            tokens = tok[pl.ds(at, per_step)].reshape(per_step * rows, depth)
            values = normed_of(tokens, vecs[0:1, :])
            product = matmul_t(values, wall[...].reshape(-1, depth)).astype(bf16)
            for c in range(per_step):
                result[at + c] = product[c * rows : (c + 1) * rows]
            start = pl.multiple_of(chip * cw // 128 * 128, 128)
            piece = tok[pl.ds(at, per_step), :, pl.ds(start, 128)].reshape(per_step * rows, 128)
            if cw < 128:
                piece = pltpu.roll(piece.astype(f32), (128 - chip * cw % 128) % 128, 1)
                piece = piece[:, :cw].astype(bf16)
            xcol[pl.ds(at, per_step)] = piece.reshape(per_step, rows, cw)
            return carry

        lax.fori_loop(0, inner // per_step, step, 0)
        each(j, lambda k: ret_copy(j, k).start())

    def ret_copy(j, k):
        return spread_copy(
            lambda l, a, b: result.at[l * inner + a * side + b], landed.at[chip], ret_s, ret_r, j, k
        )

    a_u, a_w = (tok, au_s, au_r), (tok, aw_s, aw_r)
    for j in range(1, GROUPS):
        z_copy(tok, az_s, az_r, j).wait_recv()
        u_start(*a_u, j)
        u_to_w(tok, au_s, au_r, aw_s, aw_r, j - 1)
    for i in range(3):
        swaps[i].wait()
    w_wait(*a_w, 0)
    project_in(0)
    u_to_w(tok, au_s, au_r, aw_s, aw_r, GROUPS - 1)
    landed[chip] = result[own]
    for j in range(1, GROUPS):
        w_wait(*a_w, j)
        project_in(j)
    for i in range(4, 7):
        swaps[i].start()

    def msg_copy(j, k):
        return spread_copy(lambda l, a, b: rmsg.at[own], rmsg.at[own], msg_s, msg_r, j, k)

    for j in range(GROUPS):
        each(j, lambda k: msg_copy(j, k).start())
    local[early].wait()
    for j in range(GROUPS):
        each(j, lambda k: ret_copy(j, k).wait_recv())

    pieces = max(1, 128 // cw)
    heads_of = 128 // (2 * span)
    for t in range(depth // 128):
        for i in range(3):
            tile = jnp.concatenate(
                [
                    landed[t * pieces + c][:, i * cw : i * cw + min(cw, 128)].astype(f32)
                    for c in range(pieces)
                ],
                axis=1,
            )
            to_rows(i, t * heads_of, tile)

    block = 2 * heads
    width = 4 * span
    chunks = cells // width

    def head_sum(v):
        return 0.5 * jnp.sum(v, axis=-1, keepdims=True)

    def wide(v):
        return jnp.concatenate([v, v], axis=1)

    def load_rows(ref, i):
        return jnp.concatenate(
            [ref[pl.ds(pl.multiple_of((2 * i + s) * pitch, 8), heads), :] for s in range(2)], axis=0
        )

    def gain(i):
        return jnp.concatenate([gains[i]] * 2, axis=0)

    def readout_step(i, carry):
        at = pl.multiple_of(i * block, block)
        q, k, v = (load_rows(rows_s.at[n], i) for n in range(3))
        decay = jnp.exp(-math.exp(-0.5) * jax.nn.sigmoid(load_rows(rows_s.at[3], i)))
        rate = jax.nn.sigmoid(load_rows(rows_s.at[4], i))
        erase = k * gain(0)
        erase = erase * lax.rsqrt(head_sum(erase * erase) + unit_eps)
        repl = k * (1.0 + (rate - 1.0) * gain(1))
        erase_rate = erase * rate
        erase_w, query_w = wide(erase), wide(decay * q)
        total = jnp.zeros((2 * block, 2 * span), f32)
        for c in range(chunks):
            cut = pl.ds(c * width, width)
            m = m_ref[pl.ds(at, block), cut]
            both = jnp.concatenate([(m * erase_w).astype(bf16), (m * query_w).astype(bf16)], axis=0)
            total += matmul(both, picker[cut, :])
        removed, kept = total[:block], total[block:]
        read = kept - removed * head_sum(erase_rate * q) + v * head_sum(repl * q)
        centered = read - head_sum(read) / span
        variance = head_sum(centered * centered) / span
        mixed = centered * lax.rsqrt(variance + group_eps) * gain(3)
        mixed = mixed + head_sum(q * repl * gain(2)) * v
        for s in range(2):
            cut = slice(s * heads, (s + 1) * heads)
            own_s[pl.ds(pl.multiple_of((2 * i + s) * pitch, 8), heads), :] = mixed[cut]
        rem_s[0, pl.ds(at, block), :] = removed
        rem_s[1, pl.ds(at, block), :] = decay
        rem_s[2, pl.ds(at, block), :] = erase_rate
        rem_s[3, pl.ds(at, block), :] = repl
        return carry

    lax.fori_loop(0, rows // 2, readout_step, 0)
    for h in range(heads // 2):
        first = own_s[pl.ds(2 * h, rows, stride=pitch), :]
        second = own_s[pl.ds(2 * h + 1, rows, stride=pitch), :]
        mix[own, :, 2 * h * span : 2 * (h + 1) * span] = jnp.where(low_lane, first, second).astype(
            bf16
        )

    def update_step(i, carry):
        at = pl.multiple_of(i * block, block)
        v = load_rows(rows_s.at[2], i)
        removed, decay, erase_rate, repl = (rem_s[n, pl.ds(at, block), :] for n in range(4))
        high = removed.astype(bf16).astype(f32)
        pair = jnp.where(low_lane, high, removed - high).astype(bf16)
        fresh = jnp.where(low_lane, v, 0.0).astype(bf16)
        stacked = jnp.concatenate([pair, fresh], axis=0)
        decay_w, rate_w, repl_w = wide(decay), wide(erase_rate), wide(repl)
        for c in range(chunks):
            cut = pl.ds(c * width, width)
            grown = matmul(stacked, spread[:, cut])
            m_ref[pl.ds(at, block), cut] = (
                m_ref[pl.ds(at, block), cut] * decay_w - grown[:block] * rate_w + grown[block:] * repl_w
            )
        return carry

    steps = rows // 2

    def update(start, stop):
        lax.fori_loop(start, stop, update_step, 0)

    b_u, b_w = (mix, bu_s, bu_r), (mix, bw_s, bw_r)
    for j in range(1, GROUPS):
        z_copy(mix, bz_s, bz_r, j).start()
    u_start(*b_u, 0)
    swaps[3].wait()
    for j in range(GROUPS):
        each(j, lambda k: msg_copy(j, k).wait_recv())
    update(0, steps // 4)
    for j in range(1, GROUPS):
        z_copy(mix, bz_s, bz_r, j).wait_recv()
        u_start(*b_u, j)
        u_to_w(mix, bu_s, bu_r, bw_s, bw_r, j - 1)
        update(j * steps // GROUPS, (j + 1) * steps // GROUPS)
    u_to_w(mix, bu_s, bu_r, bw_s, bw_r, GROUPS - 1)

    tiles = -(-inner // per_tile)

    def route_rows(sigma, row):
        parts = []
        for t in range(tiles):
            count = min(per_tile, inner - t * per_tile)
            total = rmsg[sigma * inner + t * per_tile, pl.ds(row, 1), :]
            for c in range(1, count):
                total += rmsg[sigma * inner + t * per_tile + c, pl.ds(row, 1), :]
            parts.append(total[:, : count * rows])
        return parts[0] if tiles == 1 else jnp.concatenate(parts, axis=1)

    def slot_copy(j, sigma):
        to = (layer + j) % GROUPS
        return rdma(
            zsrc.at[to, sigma], disp.at[own, sigma], cz_s.at[j, sigma], cz_r.at[j, sigma], dev(to, w, u)
        )

    def res_copy(j, k):
        return spread_copy(
            lambda l, a, b: rescol.at[l * inner + a * side + b], resland.at[chip], res_s, res_r, j, k
        )

    tokens_in = inner * rows
    first_expert = place * 2

    def project_out(j):
        sigma = lyr(j)
        base = sigma * inner
        tokens = mix[pl.ds(base, inner)].reshape(tokens_in, depth)
        product = matmul_t(tokens, wo[...].reshape(-1, depth)).astype(bf16)
        old = xcol[pl.ds(base, inner)].reshape(tokens_in, cw)
        res = (old.astype(f32) + product.astype(f32)).astype(bf16)
        for c in range(inner):
            rescol[base + c] = res[c * rows : (c + 1) * rows]
        codes = route_rows(sigma, 0)
        match = iota((GROUPS * slots, tokens_in), 0).astype(f32) + 1.0 == codes
        chosen_rows = matmul(jnp.where(match, 1.0, 0.0).astype(bf16), res).astype(bf16)
        for g in range(GROUPS):
            zsrc[g, sigma] = chosen_rows[g * slots : (g + 1) * slots]
        for g in range(1, GROUPS):
            slot_copy(g, sigma).start()
        disp[own, sigma] = zsrc[layer, sigma]
        ours = (
            iota((slots, tokens_in), 0).astype(f32) + (layer * slots).astype(f32) + 1.0 == codes
        )
        for e in range(2):
            held = route_rows(sigma, 8 + first_expert + e)
            sshare[e, pl.ds(pl.multiple_of(sigma * slots, slots), slots), :] = jnp.broadcast_to(
                jnp.sum(jnp.where(ours, held, 0.0), axis=1, keepdims=True), (slots, 128)
            )

    for j in range(GROUPS):
        w_wait(*b_w, j)
        project_out(j)
    for j in range(GROUPS):
        each(j, lambda k: res_copy(j, k).start())
    resland[chip] = rescol[own]

    every = GROUPS * slots
    c_u, c_w = (disp, cu_s, cu_r), (disp, cw_s, cw_r)

    def disp_u(j):
        if j:
            for s in range(GROUPS):
                slot_copy(j, s).wait_recv()
        u_start(*c_u, j)

    mblock = min(every, 128)

    def gate_up(j):
        d = lyr(j)
        k_at = pl.multiple_of(d * inner * cw, inner * cw)

        def step(i, carry):
            r_at = pl.multiple_of(i * mblock, mblock)
            parts = []
            for a in range(inner):
                ay, ax = a // side, a % side
                v = (1 - core) * a + core * (ax * side + ay)
                if every == mblock:
                    parts.append(disp[d * inner + v].reshape(every, cw))
                else:
                    parts.append(
                        disp[d * inner + v, r_at // slots, pl.ds(r_at % slots, mblock), :]
                    )
            cols = jnp.concatenate(parts, axis=1).astype(f32)
            squares = jnp.sum(cols * cols, axis=1, keepdims=True)
            cols = (cols * vecs[7:8, pl.ds(k_at, inner * cw)]).astype(bf16)
            at = pl.ds(r_at, mblock)
            squares = jnp.broadcast_to(squares, (mblock, 128))
            if j == 0:
                sshare[2, at, :] = squares
            else:
                sshare[2, at, :] += squares
            for e in range(2):
                for n, ref in enumerate((wgb, wub)):
                    cut = slice((2 * e + n) * fe, (2 * e + n + 1) * fe)
                    product = matmul(cols, ref[e, pl.ds(k_at, inner * cw), :])
                    if j == 0:
                        acc[at, cut] = product
                    else:
                        acc[at, cut] += product
            return carry

        lax.fori_loop(0, every // mblock, step, 0)

    disp_u(0)
    for j in range(1, GROUPS):
        disp_u(j)
        u_to_w(disp, cu_s, cu_r, cw_s, cw_r, j - 1)
    for i in range(early + 1, early + 4):
        local[i].wait()
    for i in range(4, 7):
        swaps[i].wait()
    w_wait(*c_w, 0)
    gate_up(0)
    u_to_w(disp, cu_s, cu_r, cw_s, cw_r, GROUPS - 1)
    for j in range(1, GROUPS):
        w_wait(*c_w, j)
        gate_up(j)

    def activate(i, carry):
        at = pl.ds(pl.multiple_of(i * mblock, mblock), mblock)
        scale = lax.rsqrt(sshare[2, at, 0:1] / depth + norm_eps)
        for e in range(2):
            gate = acc[at, 2 * e * fe : (2 * e + 1) * fe] * scale
            up = acc[at, (2 * e + 1) * fe : (2 * e + 2) * fe] * scale
            hidden = jax.nn.silu(gate) * up * sshare[e, at, 0:1]
            acc[at, e * fe : (e + 1) * fe] = hidden
        return carry

    lax.fori_loop(0, every // mblock, activate, 0)
    wide_cols = depth // 2
    step_cols = wide_cols // 2

    def sum_copy(n, k):
        a, b = k // side, k % side
        w2, u2 = (w + a) % side, (u + b) % side
        at = n * inner + k
        return rdma(
            part.at[n, w2 * side + u2], pland.at[n, k], sum_s.at[at], sum_r.at[at], dev(layer, w2, u2)
        )

    left = acc[:, 0:fe].astype(bf16)
    right = acc[:, fe : 2 * fe].astype(bf16)
    for n in range(2):
        for c in range(2):
            cut = slice(n * wide_cols + c * step_cols, n * wide_cols + (c + 1) * step_cols)
            total = matmul(left, wdb[0, :, cut]) + matmul(right, wdb[1, :, cut])
            for p in range(inner):
                piece = jnp.concatenate(
                    [
                        total[s * slots + p * half : s * slots + (p + 1) * half]
                        for s in range(GROUPS)
                    ],
                    axis=0,
                )
                part[n, p, :, c * step_cols : (c + 1) * step_cols] = piece.astype(bf16)
        for k in range(1, inner):
            sum_copy(n, k).start()

    sums = []
    for n in range(2):
        total = part[n, vp].astype(f32)
        for k in range(1, inner):
            sum_copy(n, k).wait_recv()
            total += pland[n, k].astype(f32)
        sums.append(total)
    for s in range(GROUPS):
        cut = slice(s * half, (s + 1) * half)
        retsrc[s] = jnp.concatenate([sums[0][cut], sums[1][cut]], axis=0).astype(bf16)

    def home_copy(j):
        to = (layer + j) % GROUPS
        return rdma(retsrc.at[to], rland.at[layer], home_s.at[j], home_r.at[j], dev(to, w, u))

    for j in range(1, GROUPS):
        home_copy(j).start()
    rland[layer] = retsrc[layer]
    for j in range(GROUPS):
        each(j, lambda k: res_copy(j, k).wait_recv())
    residual = jnp.concatenate([resland[c].astype(f32) for c in range(chips)], axis=1)
    find = home_col == iota((rows, GROUPS * half), 1).astype(f32)
    find = jnp.where(find, 1.0, 0.0).astype(bf16)
    for j in range(1, GROUPS):
        home_copy(j).wait_recv()
    back = [rland[g].astype(f32) for g in range(GROUPS)]
    for n in range(2):
        table = jnp.concatenate([b[n * half : (n + 1) * half] for b in back], axis=0).astype(bf16)
        cut = slice(n * wide_cols, (n + 1) * wide_cols)
        hid_ref[:, cut] = (residual[:, cut] + matmul(find, table)).astype(bf16)

    sends_done(tok, au_s, au_r, aw_s, aw_r)
    sends_done(mix, bu_s, bu_r, bw_s, bw_r)
    sends_done(disp, cu_s, cu_r, cw_s, cw_r)
    for j in range(1, GROUPS):
        z_copy(tok, az_s, az_r, j).wait_send()
        z_copy(mix, bz_s, bz_r, j).wait_send()
        home_copy(j).wait_send()
        for s in range(GROUPS):
            slot_copy(j, s).wait_send()
    for j in range(GROUPS):
        each(j, lambda k: ret_copy(j, k).wait_send())
        each(j, lambda k: msg_copy(j, k).wait_send())
        each(j, lambda k: res_copy(j, k).wait_send())
    for n in range(2):
        for k in range(1, inner):
            sum_copy(n, k).wait_send()


def local(
    latest_embeddings,
    prior_memory_grids,
    earlier_rescale_gain,
    query_map,
    lookup_map,
    content_map,
    forget_lower_map,
    forget_upper_map,
    forget_shift,
    adapt_lower_map,
    adapt_upper_map,
    adapt_shift,
    erase_lookup_gains,
    substitute_lookup_gains,
    present_extra_gains,
    attender_rescale_gain,
    result_map,
    later_rescale_gain,
    specialist_switch_maps,
    specialist_widen_maps,
    specialist_shrink_maps,
    picked_specialists,
    specialist_picked_shares,
):
    devices = lax.axis_size("ep")
    chips = devices // 2
    inner = chips // GROUPS
    side = math.isqrt(inner)
    rows, depth = latest_embeddings.shape
    _, heads, cells = prior_memory_grids.shape
    span = depth // heads
    columns = query_map.shape[1]
    cw = 2 * columns
    half = (rows + 1) // 2
    slots = inner * half
    every = GROUPS * slots
    group = devices // GROUPS
    fe = specialist_switch_maps.shape[2]
    rank = forget_lower_map.shape[1]
    padded = rows * (heads + HEAD_PAD)
    top = picked_specialists.shape[1]
    dma = pltpu.SemaphoreType.DMA
    vmem = pltpu.VMEM
    any_space = pl.BlockSpec(memory_space=pltpu.HBM)
    vector = [
        v.reshape(1, depth)
        for v in (
            earlier_rescale_gain,
            forget_shift,
            adapt_shift,
            erase_lookup_gains,
            substitute_lookup_gains,
            present_extra_gains,
            attender_rescale_gain,
            later_rescale_gain,
        )
    ]
    inputs = [
        latest_embeddings,
        prior_memory_grids.reshape(rows * heads, cells),
        query_map.T,
        lookup_map.T,
        content_map.T,
        result_map.T,
        forget_lower_map.T,
        forget_upper_map,
        adapt_lower_map.T,
        adapt_upper_map,
        *vector,
        specialist_switch_maps,
        specialist_widen_maps,
        specialist_shrink_maps,
        picked_specialists.T,
        specialist_picked_shares.T,
    ]
    relay_sems = [
        dma((GROUPS,)),
        dma((GROUPS,)),
        dma((GROUPS, side)),
        dma((GROUPS, side)),
        dma((GROUPS, side)),
        dma((GROUPS, side)),
    ]
    slot_sems = [dma((GROUPS, GROUPS)), dma((GROUPS, GROUPS))] + relay_sems[2:]
    hidden, state = pl.pallas_call(
        functools.partial(layer_kernel, devices),
        out_shape=[
            pltpu.VMEM((rows, depth), bf16),
            pltpu.VMEM((rows * heads, cells), f32),
        ],
        in_specs=[any_space] * len(inputs),
        out_specs=[pl.BlockSpec(memory_space=pltpu.VMEM)] * 2,
        scratch_shapes=[
            vmem((chips, rows, depth), bf16),
            vmem((chips, rows, depth), bf16),
            vmem((3, 2, columns, depth), bf16),
            vmem((2, columns, depth), bf16),
            vmem((4, rank, depth), bf16),
            vmem((8, depth), f32),
            vmem((top, rows), jnp.int32),
            vmem((top, rows), f32),
            vmem((2, depth, fe), bf16),
            vmem((2, depth, fe), bf16),
            vmem((2, fe, depth), bf16),
            vmem((cells, 2 * span), bf16),
            vmem((2 * span, cells), bf16),
            vmem((4, heads, 2 * span), f32),
            vmem((5, padded, 2 * span), f32),
            vmem((padded, 2 * span), f32),
            vmem((4, rows * heads, 2 * span), f32),
            vmem((chips, rows, 3 * cw), bf16),
            vmem((chips, rows, 3 * cw), bf16),
            vmem((chips, rows, cw), bf16),
            vmem((chips, rows, cw), bf16),
            vmem((chips, rows, cw), bf16),
            vmem((chips, 8 + group, 128), f32),
            vmem((GROUPS, GROUPS, slots, cw), bf16),
            vmem((chips, GROUPS, slots, cw), bf16),
            vmem((every, 4 * fe), f32),
            vmem((3, every, 128), f32),
            vmem((2, inner, GROUPS * half, depth // 2), bf16),
            vmem((2, inner, GROUPS * half, depth // 2), bf16),
            vmem((GROUPS, 2 * half, depth // 2), bf16),
            vmem((GROUPS, 2 * half, depth // 2), bf16),
            dma((24,)),
            dma((7,)),
            dma((7,)),
            *relay_sems,
            *relay_sems,
            *slot_sems,
            dma((chips,)),
            dma((chips,)),
            dma((chips,)),
            dma((chips,)),
            dma((chips,)),
            dma((chips,)),
            dma((2 * inner,)),
            dma((2 * inner,)),
            dma((GROUPS,)),
            dma((GROUPS,)),
        ],
        compiler_params=pltpu.CompilerParams(
            collective_id=0, has_side_effects=True, vmem_limit_bytes=55 * 2**20
        ),
        name="layer",
    )(*inputs)
    return hidden, state.reshape(prior_memory_grids.shape)


def solution(mesh):
    return jax.shard_map(
        local,
        mesh=mesh,
        in_specs=(
            P("ep", None),
            P("ep", None, None),
            P(),
            P(None, "ep"),
            P(None, "ep"),
            P(None, "ep"),
            P(),
            P(),
            P(),
            P(),
            P(),
            P(),
            P(),
            P(),
            P(),
            P(),
            P(None, "ep"),
            P(),
            P("ep", None, None),
            P("ep", None, None),
            P("ep", None, None),
            P("ep", None),
            P("ep", None),
        ),
        out_specs=(P("ep", None), P("ep", None, None)),
        check_vma=False,
    )
```

time: 134 us -> 82.3 us (0.61)
  the two profiles are of different devices: /device:TPU:15 before, /device:TPU:0 now
where the time goes in v1:
time: 82.3 us; the launch traced here: 82.2 us
  Pallas kernels  77.5 us (94%)
  local copies, waits for them, and re-layouts  4.03 us (5%)
    pallas_call x1, Pallas kernels, local(): pl.pallas_call(functools.partial(layer_kernel, devices), out_shape=[pltpu...  77.5 us
    unnamed x2, local copies, waits for them, and re-layouts  4.03 us

profile of v1, /device:TPU:0, one launch (start us, length us, event | category | flops | bytes accessed | tf_op | source)
XLA Modules:
  0.0 82.2 jit_solution(2192912980609132307)
XLA Ops:
  0.6 77.5 %layer.1 = (bf16[16,2048]{1,0:T(8,128)(2,1)S(1)}, f32[512,4096]{1,0:T(8,128)S(1)}) custom-call(bf16[16,2048]{1,0:T(8,128)(2,1)} %x_hbm.1, f32[512,4096]{1,0:T(8,128)} %bitcast.19, bf16[64,2048]{1,0:T(8,128)(2,1)} %bitcast.20, bf16[64,2048]{1,0:T(8,128)(2,1)} %bitcast.21, bf16[64,2048]{1,0:T(8,128)(2,1)} %bitcast.22, bf16[64,2048]{1,0:T(8,128)(2,1)} %bitcast.23, ...), custom_call_target="tpu_custom_call" | custom-call | tf_op jit(solution)/shard_map/layer/pallas_call | solution.py:705
  78.2 0.6 copy.27
  78.8 3.4 %copy.28 = f32[16,32,4096]{2,1,0:T(8,128)} copy(f32[16,32,4096]{2,1,0:T(8,128)S(1)} %bitcast.18) | data formatting | bytes 16777216
